TPU v7x, 512 devices: a whole 4x4x16 slice. The times are simulated.
512 devices in a mesh: tp: 16 (over y, x), dp: 32 (over z, core).
Axes of the slice: x: 4, y: 4, z: 16, core: 2. Of those that a mesh axis runs over, the one named last changes fastest.
Arguments:
- tokens: bfloat16 [256, 4096], P('tp', 'dp'), may hold values from -12 to 12, as said below
- norm_gain: float32 [2, 4096], P(None, 'dp'), may hold values from 0.1 to 1.9
- w_input: bfloat16 [2, 4096, 2048], P(None, 'dp', 'tp'), may hold values from -0.09375 to 0.09375
- w_gate: bfloat16 [2, 4096, 2048], P(None, 'dp', 'tp'), may hold values from -0.09375 to 0.09375
- w_recur: bfloat16 [2, 16, 128, 128], P(None, 'tp'), may hold values from -0.5 to 0.5
- w_inject: bfloat16 [2, 16, 128, 128], P(None, 'tp'), may hold values from -0.5 to 0.5
- conv_weight: bfloat16 [2, 4, 2048], P(None, None, 'tp'), may hold values from -3 to 3
- decay_param: float32 [2, 2048], P(None, 'tp'), may hold values from -2 to 5
- w_output: bfloat16 [2, 2048, 4096], P(None, 'tp', 'dp'), may hold values from -0.125 to 0.125
- lengths: int32 [256], P('dp'), may hold values from 1 to 48, 2048 in all
- conv_state: bfloat16 [2, 3, 256, 2048], P(None, None, 'dp', 'tp'), may hold values from -6 to 6
- rec_state: float32 [2, 256, 2048], P(None, 'dp', 'tp'), may hold values from -6 to 6
Outputs:
- mixed: bfloat16 [256, 4096], P('tp', 'dp')
- new_conv: bfloat16 [2, 3, 256, 2048], P(None, None, 'dp', 'tp')
- new_rec: float32 [2, 256, 2048], P(None, 'dp', 'tp')
Inputs may be any that keep to these rules, and one draw needn't show every extreme that they name: `tokens`: activations; feature scales vary.
All inputs are finite; a program needn't handle non-finite values. No bound on the sum of `lengths` on one device may be relied on, other than what follows from the above.
Results may differ from a plain program's by a relative error of at most 0.02.
Values may be sent and summed in bfloat16 or wider, within the bound.
A program may use at most 64 MiB of HBM per device.

v0:
```python
import jax
import jax.numpy as jnp
from jax import lax
from jax.sharding import PartitionSpec as P

D = 4096


EPS = 1e-06


def sent_to_all(x, axis):
    copies = jnp.broadcast_to(x, (lax.axis_size(axis), *x.shape))
    return lax.all_to_all(copies, axis, split_axis=0, concat_axis=0, tiled=True)


def in_order(tiles, dim):
    tiles = jnp.moveaxis(tiles, 0, dim)
    dims = tiles.shape
    return tiles.reshape(*dims[:dim], dims[dim] * dims[dim + 1], *dims[dim + 2 :])


def gathered_copies(x, axis, dim):
    tiles = sent_to_all(x, axis)
    return in_order(tiles, dim)


def cut_along(x, dim, count):
    before, after = (x.shape[:dim], x.shape[dim + 1 :])
    return jnp.moveaxis(x.reshape(*before, count, -1, *after), dim, 0)


def sent_and_summed(x, axis, dim):
    count = lax.axis_size(axis)
    tiles = lax.all_to_all(cut_along(x, dim, count), axis, 0, 0, tiled=True)
    return jnp.sum(tiles.astype(jnp.float32), axis=0)


def sent_together(arrays, axis, dim, along):
    columns = [a.reshape(*a.shape[:along], -1) for a in arrays]
    both = jnp.concatenate(columns, axis=along)
    result, at, finished = (sent_and_summed(both, axis, dim), 0, [])
    for a, column in zip(arrays, columns):
        piece = result[..., at : at + column.shape[along]]
        finished.append(piece.reshape(*piece.shape[:along], *a.shape[along:]))
        at += column.shape[along]
    return tuple(finished)


def body(
    tokens,
    norm_gain,
    w_input,
    w_gate,
    w_recur,
    w_inject,
    conv_weight,
    decay_param,
    w_output,
    lengths,
    conv_state,
    rec_state,
):
    state_rows = lengths.shape[0]
    live_len = lengths[:, None]
    current = tokens
    conv_list = []
    rec_list = []
    for layer_idx in range(w_input.shape[0]):
        widened = current.astype(jnp.float32)
        gathered = gathered_copies(current, "tp", 0)
        gathered_f = gathered.astype(jnp.float32)
        scaled = (gathered_f * norm_gain[layer_idx]).astype(jnp.bfloat16)
        part_value = jnp.dot(scaled, w_input[layer_idx], preferred_element_type=jnp.float32)
        part_gate = jnp.dot(scaled, w_gate[layer_idx], preferred_element_type=jnp.float32)
        part_square = jnp.sum(gathered_f * gathered_f, axis=1)
        sum_value, sum_gate, sum_square = sent_together(
            (
                part_value.astype(jnp.bfloat16),
                part_gate.astype(jnp.bfloat16),
                part_square.astype(jnp.bfloat16),
            ),
            "dp",
            0,
            1,
        )
        own_scale = lax.rsqrt(sum_square / D + EPS)
        value_in = sum_value * own_scale[:, None]
        gate_in = sum_gate * own_scale[:, None]
        conv_taps = conv_weight[layer_idx].astype(jnp.float32)
        old_taps = conv_state[layer_idx]
        tap_count = old_taps.shape[0]
        conv_out = conv_taps[tap_count] * value_in
        for back in range(1, tap_count + 1):
            conv_out = conv_out + conv_taps[tap_count - back] * jnp.where(
                back < live_len, old_taps[tap_count - back].astype(jnp.float32), jnp.float32(0.0)
            )
        local_blocks = w_recur.shape[1]
        block_width = w_recur.shape[2]
        conv_low = conv_out.astype(jnp.bfloat16).reshape(state_rows, local_blocks, block_width)
        rec_gate = jax.nn.sigmoid(
            jnp.einsum(
                "bnc,ncd->bnd", conv_low, w_recur[layer_idx], preferred_element_type=jnp.float32
            ).reshape(state_rows, -1)
        )
        inp_gate = jax.nn.sigmoid(
            jnp.einsum(
                "bnc,ncd->bnd", conv_low, w_inject[layer_idx], preferred_element_type=jnp.float32
            ).reshape(state_rows, -1)
        )
        log_decay = -8.0 * rec_gate * jax.nn.softplus(-decay_param[layer_idx])
        previous = jnp.where(live_len > 1, rec_state[layer_idx], jnp.float32(0.0))
        hidden = jnp.exp(log_decay) * previous + jnp.sqrt(-jnp.expm1(2.0 * log_decay)) * (
            inp_gate * conv_out
        )
        readout = (hidden * jax.nn.gelu(gate_in)).astype(jnp.bfloat16)
        readouts = gathered_copies(readout, "dp", 0)
        out_weight = w_output[layer_idx]
        branch = sent_and_summed(
            jnp.dot(readouts, out_weight, preferred_element_type=jnp.float32).astype(jnp.bfloat16),
            "tp",
            0,
        )
        current = (widened + branch).astype(jnp.bfloat16)
        conv_list.append(
            jnp.concatenate([old_taps[1:], value_in.astype(jnp.bfloat16)[None]], axis=0)
        )
        rec_list.append(hidden)
    return (current, jnp.stack(conv_list), jnp.stack(rec_list))


def solution(mesh):
    placed = (
        P("tp", "dp"),
        P(None, "dp"),
        P(None, "dp", "tp"),
        P(None, "dp", "tp"),
        P(None, "tp", None, None),
        P(None, "tp", None, None),
        P(None, None, "tp"),
        P(None, "tp"),
        P(None, "tp", "dp"),
        P("dp"),
        P(None, None, "dp", "tp"),
        P(None, "dp", "tp"),
    )
    return jax.shard_map(
        body,
        mesh=mesh,
        in_specs=placed,
        out_specs=(P("tp", "dp"), P(None, None, "dp", "tp"), P(None, "dp", "tp")),
        check_vma=False,
    )
```

profile of v0, /device:TPU:1, one launch (start us, length us, event | category | flops | bytes accessed | tf_op | source)
XLA Modules:
  0.0 152.4 jit_solution(12453419043310698956)
XLA Ops:
  0.6 1.3 broadcast_in_dim.69
  1.9 0.0 copy-start.6
  1.9 7.7 %all-to-all-start = ((bf16[16,16,128]{2,1,0:T(8,128)(2,1)}), bf16[16,16,128]{2,1,0:T(8,128)(2,1)S(1)}, u32[]{:S(2)}, u32[]{:S(2)}) async-start(bf16[16,16,128]{2,1,0:T(8,128)(2,1)} %broadcast_in_dim.69), calls=%async_computation | async-start | bytes 131072 | tf_op jit(solution)/shard_map/all_to_all | solution.py:14
  9.7 0.0 copy-done.6
  9.7 0.0 copy-start.8
  9.7 0.6 copy-done.8
  10.3 5.8 %all-to-all-done = bf16[16,16,128]{2,1,0:T(8,128)(2,1)S(1)} async-done(((bf16[16,16,128]{2,1,0:T(8,128)(2,1)}), bf16[16,16,128]{2,1,0:T(8,128)(2,1)S(1)}, u32[]{:S(2)}, u32[]{:S(2)}) %all-to-all-start) | async-done | bytes 65568 | tf_op jit(solution)/shard_map/all_to_all | solution.py:14
  16.2 0.0 copy-start
  16.2 0.1 fusion.24
  16.3 0.7 copy-done
  17.0 0.0 copy-start.1
  17.0 0.1 fusion
  17.2 0.7 copy-done.1
  17.9 0.1 fusion.1
  18.0 0.1 convert_element_type.208
  18.1 0.7 pad_maximum_fusion
  18.8 0.0 copy-start.7
  18.8 17.5 %all-to-all-start.1 = ((bf16[32,8,257]{2,1,0:T(8,128)(2,1)}), bf16[32,8,257]{2,1,0:T(8,128)(2,1)S(1)}, u32[]{:S(2)}, u32[]{:S(2)}) async-start(bf16[32,8,257]{2,1,0:T(8,128)(2,1)} %pad_maximum_fusion), calls=%async_computation.1 | async-start | bytes 393216 | tf_op jit(solution)/shard_map/all_to_all | solution.py:35
  36.3 0.0 copy-done.7
  36.3 0.0 copy-start.5
  36.4 0.6 copy-done.5
  37.0 0.0 copy-start.9
  37.0 18.1 %all-to-all-done.1 = bf16[32,8,257]{2,1,0:T(8,128)(2,1)S(1)} async-done(((bf16[32,8,257]{2,1,0:T(8,128)(2,1)}), bf16[32,8,257]{2,1,0:T(8,128)(2,1)S(1)}, u32[]{:S(2)}, u32[]{:S(2)}) %all-to-all-start.1) | async-done | bytes 131616 | tf_op jit(solution)/shard_map/all_to_all | solution.py:35
  55.1 0.0 copy-start.3
  55.2 0.0 copy-start.10
  55.2 0.1 fusion.73
  55.3 0.6 copy-done.3
  55.9 0.1 fusion.81
  55.9 0.0 copy-done.9
  55.9 0.0 copy-start.11
  55.9 0.1 fusion.23
  56.1 0.0 copy-done.10
  56.1 0.6 copy-done.11
  56.6 0.1 fusion.19
  56.8 0.1 fusion.91
  56.9 0.0 copy-start.2
  56.9 17.2 %all_to_all.40 = bf16[32,8,128]{2,1,0:T(8,128)(2,1)S(1)} all-to-all(bf16[32,8,128]{2,1,0:T(8,128)(2,1)S(1)} %broadcast_in_dim.74), channel_id=1, replica_groups=mesh['tp'=16,'dp'=32] {'dp'}, dimensions={0} | all-to-all | bytes 131072 | tf_op jit(solution)/shard_map/all_to_all | solution.py:14
  74.1 0.0 copy-done.2
  74.1 0.1 convolution_convert_fusion.3
  74.3 9.4 %all_to_all.41 = bf16[16,16,128]{2,1,0:T(8,128)(2,1)S(1)} all-to-all(bf16[16,16,128]{2,1,0:T(8,128)(2,1)S(1)} %bitcast.124), channel_id=1, replica_groups=mesh['tp'=16,'dp'=32] {'tp'}, dimensions={0} | all-to-all | bytes 131072 | tf_op jit(solution)/shard_map/all_to_all | solution.py:35
  83.7 0.0 copy-start.4
  83.7 0.7 copy-done.4
  84.4 9.6 %all_to_all.42 = bf16[16,16,128]{2,1,0:T(8,128)(2,1)S(1)} all-to-all(bf16[16,16,128]{2,1,0:T(8,128)(2,1)S(1)} %broadcast_in_dim.75), channel_id=1, replica_groups=mesh['tp'=16,'dp'=32] {'tp'}, dimensions={0} | all-to-all | bytes 131072 | tf_op jit(solution)/shard_map/all_to_all | solution.py:14
  94.0 0.1 fusion.26
  94.1 0.1 fusion.2
  94.3 0.1 fusion.3
  94.4 0.1 convert_element_type.209
  94.6 0.7 pad_maximum_fusion.1
  95.3 7.7 %all-to-all-start.5 = ((bf16[32,8,257]{2,1,0:T(8,128)(2,1)}), bf16[32,8,257]{2,1,0:T(8,128)(2,1)S(1)}, u32[]{:S(2)}, u32[]{:S(2)}) async-start(bf16[32,8,257]{2,1,0:T(8,128)(2,1)} %pad_maximum_fusion.1), calls=%async_computation.5 | async-start | bytes 393216 | tf_op jit(solution)/shard_map/all_to_all | solution.py:35
  103.0 18.9 %all-to-all-done.5 = bf16[32,8,257]{2,1,0:T(8,128)(2,1)S(1)} async-done(((bf16[32,8,257]{2,1,0:T(8,128)(2,1)}), bf16[32,8,257]{2,1,0:T(8,128)(2,1)S(1)}, u32[]{:S(2)}, u32[]{:S(2)}) %all-to-all-start.5) | async-done | bytes 131616 | tf_op jit(solution)/shard_map/all_to_all | solution.py:35
  122.0 0.1 fusion.70
  122.1 0.1 fusion.75
  122.2 0.1 fusion.13
  122.3 0.2 fusion.9
  122.5 0.1 fusion.90
  122.6 0.7 broadcast_in_dim.76
  123.2 4.8 %all-to-all-start.6 = ((bf16[32,8,128]{2,1,0:T(8,128)(2,1)}), bf16[32,8,128]{2,1,0:T(8,128)(2,1)S(1)}, u32[]{:S(2)}, u32[]{:S(2)}) async-start(bf16[32,8,128]{2,1,0:T(8,128)(2,1)} %broadcast_in_dim.76), calls=%async_computation.6 | async-start | bytes 131072 | tf_op jit(solution)/shard_map/all_to_all | solution.py:14
  128.1 0.6 pad_maximum_fusion.2
  128.7 12.4 %all-to-all-done.6 = bf16[32,8,128]{2,1,0:T(8,128)(2,1)S(1)} async-done(((bf16[32,8,128]{2,1,0:T(8,128)(2,1)}), bf16[32,8,128]{2,1,0:T(8,128)(2,1)S(1)}, u32[]{:S(2)}, u32[]{:S(2)}) %all-to-all-start.6) | async-done | bytes 65568 | tf_op jit(solution)/shard_map/all_to_all | solution.py:14
  141.1 0.8 convolution_convert_fusion
  141.9 3.5 %all-to-all-start.7 = ((bf16[16,16,128]{2,1,0:T(8,128)(2,1)}), bf16[16,16,128]{2,1,0:T(8,128)(2,1)S(1)}, u32[]{:S(2)}, u32[]{:S(2)}) async-start(bf16[16,16,128]{2,1,0:T(8,128)(2,1)} %bitcast.39), calls=%async_computation.7 | async-start | bytes 131072 | tf_op jit(solution)/shard_map/all_to_all | solution.py:35
  145.4 0.6 pad_maximum_fusion.3
  146.0 5.9 %all-to-all-done.7 = bf16[16,16,128]{2,1,0:T(8,128)(2,1)S(1)} async-done(((bf16[16,16,128]{2,1,0:T(8,128)(2,1)}), bf16[16,16,128]{2,1,0:T(8,128)(2,1)S(1)}, u32[]{:S(2)}, u32[]{:S(2)}) %all-to-all-start.7) | async-done | bytes 65568 | tf_op jit(solution)/shard_map/all_to_all | solution.py:35
  151.8 0.6 add_convert_fusion
  (16 shorter events, 0.2 us)
Async XLA Ops:
  1.9 7.7 %copy-start.6 = (f32[2,128]{1,0:T(2,128)S(1)}, f32[2,128]{1,0:T(2,128)}, u32[]{:S(2)}) copy-start(f32[2,128]{1,0:T(2,128)} %param.13) | copy-start | bytes 3076
  1.9 14.2 %all-to-all-start = ((bf16[16,16,128]{2,1,0:T(8,128)(2,1)}), bf16[16,16,128]{2,1,0:T(8,128)(2,1)S(1)}, u32[]{:S(2)}, u32[]{:S(2)}) async-start(bf16[16,16,128]{2,1,0:T(8,128)(2,1)} %broadcast_in_dim.69), calls=%async_computation | async-start | bytes 131072 | tf_op jit(solution)/shard_map/all_to_all | solution.py:14
  9.7 0.7 copy-start.8
  16.2 0.8 copy-start
  17.0 0.8 copy-start.1
  18.8 17.5 %copy-start.7 = (f32[2,128]{1,0:T(2,128)S(1)}, f32[2,128]{1,0:T(2,128)}, u32[]{:S(2)}) copy-start(f32[2,128]{1,0:T(2,128)} %param.19) | copy-start | bytes 3076
  18.8 36.3 %all-to-all-start.1 = ((bf16[32,8,257]{2,1,0:T(8,128)(2,1)}), bf16[32,8,257]{2,1,0:T(8,128)(2,1)S(1)}, u32[]{:S(2)}, u32[]{:S(2)}) async-start(bf16[32,8,257]{2,1,0:T(8,128)(2,1)} %pad_maximum_fusion), calls=%async_computation.1 | async-start | bytes 393216 | tf_op jit(solution)/shard_map/all_to_all | solution.py:35
  36.3 0.7 copy-start.5
  37.0 18.9 %copy-start.9 = (bf16[2,1,128,128]{3,2,1,0:T(8,128)(2,1)S(1)}, bf16[2,1,128,128]{3,2,1,0:T(8,128)(2,1)}, u32[]{:S(2)}) copy-start(bf16[2,1,128,128]{3,2,1,0:T(8,128)(2,1)} %param.16) | copy-start | bytes 196612
  55.1 0.7 copy-start.3
  55.2 0.9 copy-start.10
  55.9 0.7 copy-start.11
  56.9 17.2 %copy-start.2 = (bf16[2,128,128]{2,1,0:T(8,128)(2,1)S(1)}, bf16[2,128,128]{2,1,0:T(8,128)(2,1)}, u32[]{:S(2)}) copy-start(bf16[2,128,128]{2,1,0:T(8,128)(2,1)} %param.20) | copy-start | bytes 196612
  83.7 0.7 copy-start.4
  95.3 26.7 %all-to-all-start.5 = ((bf16[32,8,257]{2,1,0:T(8,128)(2,1)}), bf16[32,8,257]{2,1,0:T(8,128)(2,1)S(1)}, u32[]{:S(2)}, u32[]{:S(2)}) async-start(bf16[32,8,257]{2,1,0:T(8,128)(2,1)} %pad_maximum_fusion.1), calls=%async_computation.5 | async-start | bytes 393216 | tf_op jit(solution)/shard_map/all_to_all | solution.py:35
  123.2 17.9 %all-to-all-start.6 = ((bf16[32,8,128]{2,1,0:T(8,128)(2,1)}), bf16[32,8,128]{2,1,0:T(8,128)(2,1)S(1)}, u32[]{:S(2)}, u32[]{:S(2)}) async-start(bf16[32,8,128]{2,1,0:T(8,128)(2,1)} %broadcast_in_dim.76), calls=%async_computation.6 | async-start | bytes 131072 | tf_op jit(solution)/shard_map/all_to_all | solution.py:14
  141.9 9.9 %all-to-all-start.7 = ((bf16[16,16,128]{2,1,0:T(8,128)(2,1)}), bf16[16,16,128]{2,1,0:T(8,128)(2,1)S(1)}, u32[]{:S(2)}, u32[]{:S(2)}) async-start(bf16[16,16,128]{2,1,0:T(8,128)(2,1)} %bitcast.39), calls=%async_computation.7 | async-start | bytes 131072 | tf_op jit(solution)/shard_map/all_to_all | solution.py:35
where the time goes:
time: 154 us; the launch traced here: 152 us
  waiting for transfers between devices  61.1 us (40%)
  starting transfers between devices  41.2 us (27%)
  blocking collectives  36.3 us (24%)
  local copies, waits for them, and re-layouts  6.78 us (4%)
  other arithmetic  4.15 us (3%)
  matrix products  2.04 us (1%)
    all_to_all x3, waiting for transfers between devices, sent_and_summed(): tiles = lax.all_to_all(cut_along(x, dim, count), axis, 0, 0, tiled=True)  42.9 us
    all_to_all x3, starting transfers between devices, sent_and_summed(): tiles = lax.all_to_all(cut_along(x, dim, count), axis, 0, 0, tiled=True)  28.7 us
    all_to_all x2, blocking collectives, sent_to_all(): return lax.all_to_all(copies, axis, split_axis=0, concat_axis=0, tiled=True)  26.8 us
    all_to_all x2, waiting for transfers between devices, sent_to_all(): return lax.all_to_all(copies, axis, split_axis=0, concat_axis=0, tiled=True)  18.2 us
    all_to_all x2, starting transfers between devices, sent_to_all(): return lax.all_to_all(copies, axis, split_axis=0, concat_axis=0, tiled=True)  12.5 us
    all_to_all x1, blocking collectives, sent_and_summed(): tiles = lax.all_to_all(cut_along(x, dim, count), axis, 0, 0, tiled=True)  9.42 us
    unnamed x24, local copies, waits for them, and re-layouts  4.53 us
  transfers between devices with their start and end apart: 5, of which 5 were waited for; matrix products, arithmetic and copies ran while one was open for 1% of the time, Pallas kernels for 0%

commit v1 on v0

v1 whole, which is shorter than its diff:
```python
import functools

import jax
import jax.numpy as jnp
from jax import lax
from jax.experimental import pallas as pl
from jax.experimental.pallas import tpu as pltpu
from jax.sharding import PartitionSpec as P

EPS = 1e-06
MESH = pl.DeviceIdType.MESH
BF = jnp.bfloat16
F32 = jnp.float32
LN = 128


def tp_peer(nt, me, j):
    if nt != 16:
        return lax.rem(me + j + 1, nt)
    i = j + j // 10
    y = (me // 4 + 2 + i // 4) % 4
    x = (me + 2 + i % 4) % 4
    return y * 4 + x


def dp_peer(nd, me, j):
    nz = nd // 2
    i = j // 2
    z = (me // 2 + nz // 2 + ((i + 1) // 2) * (2 * (i % 2) - 1) + nz) % nz
    return z * 2 + j % 2


def one_less_exp(y):
    near = -y * (1.0 + y * (1 / 2 + y * (1 / 6 + y * (1 / 24 + y * (1 / 120)))))
    return jnp.where(y > -0.1, near, 1.0 - jnp.exp(y))


def kernel(nt, nd, tr, sr, lens, tok, gain, win, wgate, wrec, winj, cw, dec, wout, cs, rs,
           mixed, nconv, nrec,
           x_v, gain_v, wcat, rcat, cw_v, dec_v, wout_v, cs_v, rs_v,
           xg, pb, rb, ssb, ssr, ro, rg, ob, og, x1, nconv_v, nrec_v,
           ssem, rsem, lsem, osem):
    t = lax.axis_index("tp")
    d = lax.axis_index("dp")
    nr = nt * tr
    width = nd * LN

    loads = [
        pltpu.make_async_copy(tok, x_v, lsem.at[0]),
        pltpu.make_async_copy(gain, gain_v, lsem.at[1]),
        pltpu.make_async_copy(win, wcat.at[:, :, pl.ds(0, LN)], lsem.at[2]),
        pltpu.make_async_copy(wgate, wcat.at[:, :, pl.ds(LN, LN)], lsem.at[3]),
        pltpu.make_async_copy(wrec.at[:, 0], rcat.at[:, :, pl.ds(0, LN)], lsem.at[4]),
        pltpu.make_async_copy(winj.at[:, 0], rcat.at[:, :, pl.ds(LN, LN)], lsem.at[5]),
        pltpu.make_async_copy(cw, cw_v, lsem.at[6]),
        pltpu.make_async_copy(dec, dec_v, lsem.at[7]),
        pltpu.make_async_copy(wout, wout_v, lsem.at[8]),
        pltpu.make_async_copy(cs, cs_v, lsem.at[9]),
        pltpu.make_async_copy(rs, rs_v, lsem.at[10]),
    ]
    for c in loads:
        c.start()

    barrier = pltpu.get_barrier_semaphore()

    def sig_dp(j, _):
        pl.semaphore_signal(barrier, inc=1, device_id={"dp": dp_peer(nd, d, j)}, device_id_type=MESH)
        return 0

    def sig_tp(j, _):
        pl.semaphore_signal(barrier, inc=1, device_id={"tp": tp_peer(nt, t, j)}, device_id_type=MESH)
        return 0

    lax.fori_loop(0, nd - 2, sig_dp, 0)
    pl.semaphore_signal(barrier, inc=1, device_id={"dp": d + 1 - 2 * (d % 2)}, device_id_type=MESH)
    lax.fori_loop(0, nt - 1, sig_tp, 0)
    pl.semaphore_wait(barrier, nt + nd - 2)

    def remote(src, dst, s, dev):
        return pltpu.make_async_remote_copy(
            src_ref=src, dst_ref=dst, send_sem=ssem.at[s], recv_sem=rsem.at[s],
            device_id=dev, device_id_type=MESH)

    def send_tp(src_of, dst, s):
        def step(j, _):
            p = tp_peer(nt, t, j)
            remote(src_of(p), dst, s, {"tp": p}).start()
            return 0
        lax.fori_loop(0, nt - 1, step, 0)

    def send_dp(copies):
        def one(p):
            for src_of, dst, s in copies:
                remote(src_of(p), dst, s, {"dp": p}).start()

        def step(j, _):
            one(dp_peer(nd, d, j))
            return 0
        lax.fori_loop(0, nd - 2, step, 0)
        one(d + 1 - 2 * (d % 2))

    def tp_wait(buf, s):
        return remote(buf.at[pl.ds(0, nt - 1)], buf.at[pl.ds(0, nt - 1)], s, {"tp": t})

    def dp_wait(buf, s):
        return remote(buf.at[pl.ds(0, nd - 1)], buf.at[pl.ds(0, nd - 1)], s, {"dp": d})

    row8 = lax.broadcasted_iota(jnp.int32, (sr, LN), 0)
    lane8 = lax.broadcasted_iota(jnp.int32, (sr, LN), 1)
    live = jnp.zeros((sr, LN), jnp.int32)
    for i in range(sr):
        live = jnp.where(row8 == i, lens[i], live)

    loads[0].wait()
    cur = x_v
    for l in range(2):
        q = 5 * l
        send_tp(lambda p: cur, xg.at[l, t], q)
        xg[l, t] = cur[...]
        if l == 0:
            for c in loads[1:]:
                c.wait()
        tp_wait(xg.at[l], q).wait_recv()
        xf = xg[l].reshape(nr, LN).astype(F32)
        scaled = (xf * gain_v[l][None, :]).astype(BF)
        part = jnp.dot(scaled, wcat[l], preferred_element_type=F32)
        pb[l] = part.reshape(nd, sr, 2 * LN).astype(BF)
        sq = xf * xf
        hi = sq.astype(BF)
        lo = (sq - hi.astype(F32)).astype(BF)
        ones = jnp.ones((8, LN), BF)
        dn = (((1,), (1,)), ((), ()))
        st = (lax.dot_general(ones, hi, dn, preferred_element_type=F32)
              + lax.dot_general(ones, lo, dn, preferred_element_type=F32))
        if nr < LN:
            st = jnp.concatenate([st, jnp.zeros((8, LN - nr), F32)], axis=1)
        for k in range(max(nr // LN, 1)):
            ssb[l, k] = st[0:1, k * LN:(k + 1) * LN]
        per = LN // sr
        send_dp([
            (lambda p: pb.at[l, p], rb.at[l, d], q + 1),
            (lambda p: ssb.at[l, p // per], ssr.at[l, d], q + 2),
        ])
        rb[l, d] = pb[l, d]
        ssr[l, d] = ssb[l, d // per]

        taps = cw_v[l].astype(F32)
        nt_taps = taps.shape[0] - 1
        past = jnp.zeros((sr, LN), F32)
        for back in range(1, nt_taps + 1):
            past = past + taps[nt_taps - back:nt_taps - back + 1] * jnp.where(
                live > back, cs_v[l, nt_taps - back].astype(F32), 0.0)
        previous = jnp.where(live > 1, rs_v[l], 0.0)
        soft = jax.nn.softplus(-dec_v[l:l + 1])

        dp_wait(rb.at[l], q + 1).wait_recv()
        dp_wait(ssr.at[l], q + 2).wait_recv()
        acc = jnp.sum(rb[l].astype(F32), axis=0)
        sst = jnp.sum(ssr[l], axis=0)
        ss = jnp.sum(jnp.where(lane8 == row8 + sr * (d % per), sst, 0.0), axis=1, keepdims=True)
        scale = lax.rsqrt(ss / width + EPS)
        value = acc[:, :LN] * scale
        gate = acc[:, LN:] * scale
        conv = taps[nt_taps:] * value + past
        gg = jax.nn.sigmoid(jnp.dot(conv.astype(BF), rcat[l], preferred_element_type=F32))
        log_decay = -8.0 * gg[:, :LN] * soft
        hidden = jnp.exp(log_decay) * previous + jnp.sqrt(one_less_exp(2.0 * log_decay)) * (
            gg[:, LN:] * conv)
        ro[l] = (hidden * jax.nn.gelu(gate)).astype(BF)
        send_dp([(lambda p: ro.at[l], rg.at[l, d], q + 3)])
        rg[l, d] = ro[l]
        for m in range(nt_taps - 1):
            nconv_v[l, m] = cs_v[l, m + 1]
        nconv_v[l, nt_taps - 1] = value.astype(BF)
        nrec_v[l] = hidden
        pltpu.make_async_copy(nconv_v.at[l], nconv.at[l], osem.at[0]).start()
        pltpu.make_async_copy(nrec_v.at[l], nrec.at[l], osem.at[1]).start()

        dp_wait(rg.at[l], q + 3).wait_recv()
        out = jnp.dot(rg[l].astype(F32).reshape(nr, LN).astype(BF), wout_v[l], preferred_element_type=F32)
        ob[l] = out.reshape(nt, tr, LN).astype(BF)
        send_tp(lambda p: ob.at[l, p], og.at[l, t], q + 4)
        og[l, t] = ob[l, t]
        tp_wait(og.at[l], q + 4).wait_recv()
        branch = jnp.sum(og[l].astype(F32), axis=0)
        x1[l] = (cur[...].astype(F32) + branch).astype(BF)
        cur = x1.at[l]

    last = pltpu.make_async_copy(x1.at[1], mixed, osem.at[2])
    last.start()
    for l in range(2):
        q = 5 * l
        tp_wait(xg.at[l], q).wait_send()
        dp_wait(rb.at[l], q + 1).wait_send()
        dp_wait(ssr.at[l], q + 2).wait_send()
        dp_wait(rg.at[l], q + 3).wait_send()
        tp_wait(og.at[l], q + 4).wait_send()
    pltpu.make_async_copy(nconv_v, nconv, osem.at[0]).wait()
    pltpu.make_async_copy(nrec_v, nrec, osem.at[1]).wait()
    last.wait()


def solution(mesh):
    nt, nd = mesh.shape["tp"], mesh.shape["dp"]

    def body(tokens, norm_gain, w_input, w_gate, w_recur, w_inject, conv_weight, decay_param,
             w_output, lengths, conv_state, rec_state):
        tr, sr = tokens.shape[0], lengths.shape[0]
        anyspec = pl.BlockSpec(memory_space=pl.ANY)
        V = pltpu.VMEM
        return pl.pallas_call(
            functools.partial(kernel, nt, nd, tr, sr),
            out_shape=(
                jax.ShapeDtypeStruct(tokens.shape, BF),
                jax.ShapeDtypeStruct(conv_state.shape, BF),
                jax.ShapeDtypeStruct(rec_state.shape, F32),
            ),
            in_specs=[pl.BlockSpec(memory_space=pltpu.SMEM)] + [anyspec] * 11,
            out_specs=(anyspec,) * 3,
            scratch_shapes=[
                V((tr, LN), BF), V((2, LN), F32), V((2, LN, 2 * LN), BF), V((2, LN, 2 * LN), BF),
                V(conv_weight.shape, BF), V((2, LN), F32), V((2, LN, LN), BF),
                V(conv_state.shape, BF), V(rec_state.shape, F32),
                V((2, nt, tr, LN), BF), V((2, nd, sr, 2 * LN), BF), V((2, nd, sr, 2 * LN), BF),
                V((2, max(nt * tr // LN, 1), 1, LN), F32), V((2, nd, 1, LN), F32),
                V((2, sr, LN), BF), V((2, nd, sr, LN), BF),
                V((2, nt, tr, LN), BF), V((2, nt, tr, LN), BF), V((2, tr, LN), BF),
                V(conv_state.shape, BF), V(rec_state.shape, F32),
                pltpu.SemaphoreType.DMA((10,)), pltpu.SemaphoreType.DMA((10,)),
                pltpu.SemaphoreType.DMA((11,)), pltpu.SemaphoreType.DMA((3,)),
            ],
            compiler_params=pltpu.CompilerParams(collective_id=0, has_side_effects=True),
        )(lengths, tokens, norm_gain, w_input, w_gate, w_recur, w_inject, conv_weight, decay_param,
          w_output, conv_state, rec_state)

    placed = (
        P("tp", "dp"),
        P(None, "dp"),
        P(None, "dp", "tp"),
        P(None, "dp", "tp"),
        P(None, "tp", None, None),
        P(None, "tp", None, None),
        P(None, None, "tp"),
        P(None, "tp"),
        P(None, "tp", "dp"),
        P("dp"),
        P(None, None, "dp", "tp"),
        P(None, "dp", "tp"),
    )
    return jax.shard_map(
        body,
        mesh=mesh,
        in_specs=placed,
        out_specs=(P("tp", "dp"), P(None, None, "dp", "tp"), P(None, "dp", "tp")),
        check_vma=False,
    )
```

time: 154 us -> 73.2 us (0.48)
  Pallas kernels: 0 us -> 69.7 us
  waiting for transfers between devices: 61.1 us -> 0 us
  starting transfers between devices: 41.2 us -> 0 us
  blocking collectives: 36.3 us -> 0 us
  local copies, waits for them, and re-layouts: 6.78 us -> 2.58 us
  other arithmetic: 4.15 us -> 0 us
  matrix products: 2.04 us -> 0 us
    pallas_call x0 -> x1, Pallas kernels: none -> 69.7 us  [body(): pl.pallas_call(functools.partial(kernel, nt, nd, tr, sr), out_shape=(jax....]
    all_to_all x5 -> x0, waiting for transfers between devices: 61.1 us -> none  [the longest x3 42.9 us: sent_and_summed(): tiles = lax.all_to_all(cut_along(x, dim, count), axis, 0, 0, tiled=True)]
    all_to_all x5 -> x0, starting transfers between devices: 41.2 us -> none  [the longest x3 28.7 us: sent_and_summed(): tiles = lax.all_to_all(cut_along(x, dim, count), axis, 0, 0, tiled=True)]
    all_to_all x3 -> x0, blocking collectives: 36.3 us -> none  [the longest x2 26.8 us: sent_to_all(): return lax.all_to_all(copies, axis, split_axis=0, concat_axis=0, tiled=True)]
    dot_general x10 -> x0, matrix products: 2.04 us -> none  [the longest x2 0.91 us: body(): jnp.dot(readouts, out_weight, preferred_element_type=jnp.float32)]
    broadcast_in_dim x4 -> x0, local copies, waits for them, and re-layouts: 2 us -> none  [sent_to_all(): copies = jnp.broadcast_to(x, (lax.axis_size(axis), *x.shape))]
    unnamed x24 -> x7, local copies, waits for them, and re-layouts: 4.53 us -> 2.58 us
  transfers between devices with their start and end apart: 5 -> 0, of which waited for: 5 -> 0; matrix products, arithmetic and copies ran while one was open for 1% -> 0% of each run, Pallas kernels for 0% -> 0%
where the time goes in v1:
time: 73.2 us; the launch traced here: 73 us
  Pallas kernels  69.7 us (95%)
  local copies, waits for them, and re-layouts  2.58 us (4%)
    pallas_call x1, Pallas kernels, body(): pl.pallas_call(functools.partial(kernel, nt, nd, tr, sr), out_shape=(jax....  69.7 us
    unnamed x7, local copies, waits for them, and re-layouts  2.58 us

profile of v1, /device:TPU:1, one launch (start us, length us, event | category | flops | bytes accessed | tf_op | source)
XLA Modules:
  0.0 73.0 jit_solution(9762384397256944037)
XLA Ops:
  0.6 69.7 %shard_map.139 = (bf16[16,128]{1,0:T(8,128)(2,1)}, bf16[2,3,8,128]{3,2,1,0:T(8,128)(2,1)}, f32[2,8,128]{2,1,0:T(8,128)}) custom-call(s32[8]{0:T(128)} %lens.1, bf16[16,128]{1,0:T(8,128)(2,1)} %tok.1, f32[2,128]{1,0:T(2,128)} %gain.1, bf16[2,128,128]{2,1,0:T(8,128)(2,1)} %win.1, bf16[2,128,128]{2,1,0:T(8,128)(2,1)} %wgate.1, bf16[2,1,128,128]{3,2,1,0:T(8,128)(2,1)} %wrec.1, ...), custom_call_target="tpu_custom_call" | custom-call | tf_op jit(solution)/shard_map/pallas_call | solution.py:211
  70.4 0.0 copy-start
  70.4 1.3 %copy.18 = bf16[16,128]{1,0:T(8,128)(2,1)} copy(bf16[16,128]{1,0:T(8,128)(2,1)} %get-tuple-element.6) | data formatting | bytes 8192
  71.7 0.0 copy-done
  71.7 0.0 copy-start.1
  71.7 0.6 copy.19
  72.3 0.1 copy-done.1
  72.4 0.6 copy.20
Async XLA Ops:
  70.4 1.3 %copy-start = (bf16[2,3,8,128]{3,2,1,0:T(8,128)(2,1)S(1)}, bf16[2,3,8,128]{3,2,1,0:T(8,128)(2,1)}, u32[]{:S(2)}) copy-start(bf16[2,3,8,128]{3,2,1,0:T(8,128)(2,1)} %get-tuple-element.7) | copy-start | bytes 36868
  71.7 0.7 copy-start.1
